TPU v7x, 32 devices: a whole 2x2x4 slice. The times are simulated.
32 devices in a mesh: sp: 8 (over z, x), tp: 4 (over y, core).
Axes of the slice: x: 2, y: 2, z: 4, core: 2. Of those that a mesh axis runs over, the one named last changes fastest.
Arguments:
- queries: bfloat16 [8192, 1536], P('sp', 'tp'), may hold values from -200 to 200
- key_heads: bfloat16 [8192, 512], P('sp', 'tp'), may hold values from -6 to 6
- projected_value_heads: bfloat16 [8192, 512], P('sp', 'tp'), may hold values from -5 to 5
- sink_logit_table: float32 [24], P('tp'), may hold values from 0 to 4
- out_weight: bfloat16 [1536, 3072], P('tp'), may hold values from -1.5 to 1.5
- residual: bfloat16 [8192, 3072], P('sp', 'tp'), may hold values from -16 to 16
- norm_gain: bfloat16 [3072], P('tp'), may hold values from 0.099609375 to 1.8984375
- up_weight: bfloat16 [3072, 12288], P('sp', 'tp'), may hold values from -0.109375 to 0.109375
- down_weight: bfloat16 [12288, 3072], P('tp', 'sp'), may hold values from -0.0546875 to 0.0546875
Outputs:
- result: bfloat16 [8192, 3072], P('sp', 'tp')
All inputs are finite; a program needn't handle non-finite values.
Results may differ from a plain program's by a relative error of at most 0.015.
Values may be sent and summed in bfloat16 or wider, within the bound.
No kernel may reach another device: no remote copies, remote signals or barrier semaphores. Data moves between devices by JAX's collectives and lax.ppermute only.
A program may use at most 128 MiB of HBM per device.

v0:
```python
import jax
import jax.numpy as jnp
from jax import lax
from jax.sharding import PartitionSpec as P

D = 3072
HEAD_SIZE = 64
WINDOW_SPAN = 128
epsilon = 1e-06


def shifted(block, axis, distance):
    devices = range(lax.axis_size(axis))
    route = [(i - distance, i) for i in devices if i - distance in devices]
    return lax.ppermute(block, axis, route)


def attend(queries, key_heads, projected_value_heads, sink_logit_table, previous, offset):
    row_count = queries.shape[0]
    kv_cols = key_heads.shape[1]
    kv_local = kv_cols // HEAD_SIZE
    group_count = queries.shape[1] // kv_cols
    block_count = row_count // WINDOW_SPAN
    extended_keys = jnp.concatenate([previous[:, :kv_cols], key_heads], axis=0)
    extended_values = jnp.concatenate([previous[:, kv_cols:], projected_value_heads], axis=0)

    def banded(source_rows):
        shaped = source_rows.reshape(block_count + 1, WINDOW_SPAN, kv_local, HEAD_SIZE)
        return jnp.concatenate([shaped[:-1], shaped[1:]], axis=1)

    key_band = banded(extended_keys)
    value_band = banded(extended_values)
    query_block_list = queries.reshape(block_count, WINDOW_SPAN, kv_local, group_count, HEAD_SIZE)
    scores = jnp.einsum(
        "nqkgd,nskd->nkgqs", query_block_list, key_band, preferred_element_type=jnp.float32
    ) * HEAD_SIZE ** (-0.5)
    within = jnp.arange(WINDOW_SPAN)[:, None]
    column = jnp.arange(2 * WINDOW_SPAN)[None, :]
    distance = WINDOW_SPAN + within - column
    valid = (distance >= 0) & (distance < WINDOW_SPAN)
    key_pos = (
        offset
        + jnp.arange(block_count)[:, None] * WINDOW_SPAN
        + jnp.arange(2 * WINDOW_SPAN)[None, :]
        - WINDOW_SPAN
    )
    allowed = valid[None] & (key_pos >= 0)[:, None, :]
    allowed = allowed[:, None, None]
    head_sink_logit = sink_logit_table.reshape(kv_local, group_count)[None, :, :, None, None]
    masked = jnp.where(allowed, scores, -1e30)
    ceiling = jnp.maximum(jnp.max(masked, axis=-1, keepdims=True), head_sink_logit)
    powers = jnp.where(allowed, jnp.exp(masked - ceiling), 0.0)
    denom = jnp.sum(powers, axis=-1, keepdims=True) + jnp.exp(head_sink_logit - ceiling)
    probs = (powers / denom).astype(jnp.bfloat16)
    output = jnp.einsum("nkgqs,nskd->nqkgd", probs, value_band, preferred_element_type=jnp.float32)
    return output.astype(jnp.bfloat16).reshape(row_count, queries.shape[1])


def rounded(values):
    return lax.optimization_barrier(values.astype(jnp.bfloat16)).astype(jnp.float32)


def body(
    queries,
    key_heads,
    projected_value_heads,
    sink_logit_table,
    out_weight,
    residual,
    norm_gain,
    up_weight,
    down_weight,
):
    row_count = queries.shape[0]
    offset = lax.axis_index("sp") * row_count
    tail = jnp.concatenate(
        [key_heads[row_count - WINDOW_SPAN :], projected_value_heads[row_count - WINDOW_SPAN :]],
        axis=1,
    )
    previous = shifted(tail, "sp", 1)
    attended = attend(queries, key_heads, projected_value_heads, sink_logit_table, previous, offset)
    partial_value = rounded(jnp.dot(attended, out_weight, preferred_element_type=jnp.float32))
    mixed_sum = lax.psum_scatter(
        partial_value.astype(jnp.bfloat16), "tp", scatter_dimension=1, tiled=True
    ).astype(jnp.float32)
    stream = rounded(residual.astype(jnp.float32) + mixed_sum)
    squares = lax.psum(jnp.sum(stream * stream, axis=1, keepdims=True), "tp")
    normed = (stream * lax.rsqrt(squares / D + epsilon) * norm_gain.astype(jnp.float32)).astype(
        jnp.bfloat16
    )
    normed_whole = lax.all_gather(normed, "tp", axis=1, tiled=True)
    hidden_pre = jnp.dot(
        normed_whole,
        lax.all_gather(up_weight, "sp", axis=0, tiled=True),
        preferred_element_type=jnp.float32,
    )
    activated = jnp.square(jax.nn.relu(hidden_pre)).astype(jnp.bfloat16)
    terms = jnp.dot(
        activated,
        lax.all_gather(down_weight, "sp", axis=1, tiled=True),
        preferred_element_type=jnp.float32,
    )
    branch_sum = lax.psum_scatter(
        rounded(terms).astype(jnp.bfloat16), "tp", scatter_dimension=1, tiled=True
    ).astype(jnp.float32)
    return (stream + branch_sum).astype(jnp.bfloat16)


def solution(mesh):
    return jax.shard_map(
        body,
        mesh=mesh,
        in_specs=(
            P("sp", "tp"),
            P("sp", "tp"),
            P("sp", "tp"),
            P("tp"),
            P("tp", None),
            P("sp", "tp"),
            P("tp"),
            P("sp", "tp"),
            P("tp", "sp"),
        ),
        out_specs=P("sp", "tp"),
        check_vma=False,
    )
```

profile of v0, /device:TPU:0, one launch (start us, length us, event | category | flops | bytes accessed | tf_op | source)
XLA Modules:
  0.0 985.8 jit_solution(6724844009850247608)
XLA Ops:
  6.5 0.9 slice.32
  7.5 0.8 slice.33
  8.2 4.9 collective-permute-start
  13.2 0.1 add_compare_fusion
  13.3 1.0 broadcast_and_fusion
  14.3 2.0 reshape.91
  16.3 2.0 reshape.89
  18.3 1.4 copy.20
  19.7 1.1 copy.35
  20.8 1.9 copy.19
  22.7 0.7 max.26
  23.4 1.9 copy.15
  25.3 1.7 pad_maximum_fusion
  27.0 1.2 reshape.90
  28.2 1.0 copy.18
  29.2 2.5 fusion
  31.7 0.1 broadcast_maximum_fusion
  31.7 2.6 copy-done.3
  34.3 2.8 fusion.1
  37.1 0.1 exponential_add_fusion
  37.2 0.2 reshape.88
  37.5 0.4 copy.14
  37.9 4.9 fusion.8
  42.7 0.5 copy.23
  43.3 0.0 copy-start.6
  43.3 5.4 convolution_convert_fusion.1
  48.7 0.0 reduce-scatter.3.cloned.1.call-update
  48.7 0.0 all-gather.4.cloned.1.call-start
  48.8 58.3 %reduce-scatter.3.cloned.1.call-done = bf16[1024,768]{1,0:T(8,128)(2,1)} async-done(((bf16[1024,3072]{1,0:T(8,128)(2,1)}), bf16[1024,768]{1,0:T(8,128)(2,1)}) %reduce-scatter.3.cloned.1.call-update) | async-done | bytes 1572880 | tf_op jit(solution)/shard_map/reduce_scatter | solution.py:83
  107.1 2.3 add_convert_fusion
  109.3 0.0 copy-start.2
  109.3 0.4 fusion.2
  109.7 5.8 psum.7
  115.5 1.5 fusion.4
  117.0 0.0 all-gather.4.cloned.1.call-update
  117.1 0.0 all-gather.6.cloned.1.call-start
  117.1 0.7 all-gather.6.cloned.1.call-update
  117.8 0.0 all-gather.8.cloned.1.call-start
  117.9 0.5 all-gather.8.cloned.1.call-update
  118.4 0.2 reduce-scatter.5.cloned.1.call-start
  118.6 45.6 %all-gather.4.cloned.1.call-done = bf16[1024,3072]{1,0:T(8,128)(2,1)} async-done(((bf16[1024,768]{1,0:T(8,128)(2,1)}), bf16[1024,3072]{1,0:T(8,128)(2,1)}) %all-gather.4.cloned.1.call-update) | async-done | bytes 6291472 | tf_op jit(solution)/shard_map/all_gather | solution.py:91
  164.2 364.0 %all-gather.6.cloned.1.call-done = bf16[3072,3072]{1,0:T(8,128)(2,1)} async-done(((bf16[384,3072]{1,0:T(8,128)(2,1)}), bf16[3072,3072]{1,0:T(8,128)(2,1)}) %all-gather.6.cloned.1.call-update) | async-done | bytes 18874384 | tf_op jit(solution)/shard_map/all_gather | solution.py:94
  528.2 25.8 %multiply_convert_fusion.clone.4 = bf16[1024,3072]{1,0:T(8,128)(2,1)} fusion(bf16[1024,3072]{1,0:T(8,128)(2,1)} %all-gather.4.cloned.1.call-done, bf16[3072,3072]{1,0:T(8,128)(2,1)} %all-gather.6.cloned.1.call-done), kind=kOutput, calls=%fused_computation.clone.clone.clone.1 | convolution fusion | flops 19336790016 | bytes 31457280 | tf_op jit(solution)/shard_map/dot_general | solution.py:92
  553.9 338.0 %all-gather.8.cloned.1.call-done = bf16[3072,3072]{1,0:T(8,128)(2,1)} async-done(((bf16[3072,384]{1,0:T(8,128)(2,1)}), bf16[3072,3072]{1,0:T(8,128)(2,1)}) %all-gather.8.cloned.1.call-update) | async-done | bytes 18874384 | tf_op jit(solution)/shard_map/all_gather | solution.py:100
  892.0 25.8 %convolution_convert_fusion = bf16[1024,3072]{1,0:T(8,128)(2,1)} fusion(bf16[3072,3072]{1,0:T(8,128)(2,1)} %all-gather.8.cloned.1.call-done, bf16[1024,3072]{1,0:T(8,128)(2,1)} %multiply_convert_fusion.clone.4), kind=kOutput, calls=%fused_computation.4 | convolution fusion | flops 19330498560 | bytes 31457280 | tf_op jit(solution)/shard_map/dot_general | solution.py:98
  917.8 0.0 reduce-scatter.5.cloned.1.call-update
  917.9 58.0 %reduce-scatter.5.cloned.1.call-done = bf16[1024,768]{1,0:T(8,128)(2,1)} async-done(((bf16[1024,3072]{1,0:T(8,128)(2,1)}), bf16[1024,768]{1,0:T(8,128)(2,1)}) %reduce-scatter.5.cloned.1.call-update) | async-done | bytes 1572880 | tf_op jit(solution)/shard_map/reduce_scatter | solution.py:103
  975.9 3.4 fusion.5
  (20 shorter events, 0.1 us)
Async XLA Ops:
  6.5 36.7 %copy-start = (bf16[384,3072]{1,0:T(8,128)(2,1)S(1)}, bf16[384,3072]{1,0:T(8,128)(2,1)}, u32[]{:S(2)}) copy-start(bf16[384,3072]{1,0:T(8,128)(2,1)} %param.13) | copy-start | bytes 7077892
  6.5 18.8 %copy-start.4 = (bf16[1024,128]{1,0:T(8,128)(2,1)S(1)}, bf16[1024,128]{1,0:T(8,128)(2,1)}, u32[]{:S(2)}) copy-start(bf16[1024,128]{1,0:T(8,128)(2,1)} %param.10) | copy-start | bytes 786436
  6.5 100.5 %reduce-scatter.3.cloned.1.call-start = ((), (), s32[]{:S(2)}) async-start(), calls=%async_computation.2 | async-start | bytes 7864320 | tf_op jit(solution)/shard_map/reduce_scatter | solution.py:83
  8.2 17.1 %collective-permute-start = (bf16[128,256]{1,0:T(8,128)(2,1)S(1)}, bf16[128,256]{1,0:T(8,128)(2,1)S(1)}, u32[]{:S(2)}, u32[]{:S(2)}) collective-permute-start(bf16[128,256]{1,0:T(8,128)(2,1)S(1)} %pad_maximum_fusion.2), channel_id=1, source_target_pairs={{0,4},{4,8},{8,12},{12,16},{16,20},{20,24},{24,28},{1,5},{5,9},{9,... | collective-permute-start | bytes 196616 | tf_op jit(solution)/shard_map/ppermute | solution.py:15
  29.1 8.7 copy-start.5
  31.6 2.7 copy-start.3
  43.3 5.5 copy-start.6
  48.7 115.5 %all-gather.4.cloned.1.call-start = ((), (), s32[]{:S(2)}) async-start(), calls=%async_computation.3 | async-start | bytes 7864320 | tf_op jit(solution)/shard_map/all_gather | solution.py:91
  109.3 444.6 %copy-start.2 = (bf16[1024,768]{1,0:T(8,128)(2,1)}, bf16[1024,768]{1,0:T(8,128)(2,1)S(1)}, u32[]{:S(2)}) copy-start(bf16[1024,768]{1,0:T(8,128)(2,1)S(1)} %add_convert_fusion) | copy-start | bytes 4718596
  117.1 411.1 %all-gather.6.cloned.1.call-start = ((), (), s32[]{:S(2)}) async-start(), calls=%async_computation.4 | async-start | bytes 21233664 | tf_op jit(solution)/shard_map/all_gather | solution.py:94
  117.8 774.2 %all-gather.8.cloned.1.call-start = ((), (), s32[]{:S(2)}) async-start(), calls=%async_computation.5 | async-start | bytes 21233664 | tf_op jit(solution)/shard_map/all_gather | solution.py:100
  118.4 857.5 %reduce-scatter.5.cloned.1.call-start = ((), (), s32[]{:S(2)}) async-start(), calls=%async_computation.6 | async-start | bytes 7864320 | tf_op jit(solution)/shard_map/reduce_scatter | solution.py:103
  892.0 87.3 %copy-start.1 = (bf16[384,3072]{1,0:T(8,128)(2,1)S(1)}, bf16[384,3072]{1,0:T(8,128)(2,1)}, u32[]{:S(2)}) copy-start(bf16[384,3072]{1,0:T(8,128)(2,1)} %param.13) | copy-start | bytes 7077892
Sparse Core Ops, SparseCore 0:
  48.8 58.1 reduce-scatter.2
  117.2 46.9 all-gather.3
  165.8 362.3 all-gather.5
  529.6 362.3 all-gather.7
  918.0 57.8 reduce-scatter.4
where the time goes:
time: 986 us
  waiting for transfers between devices  865 us (88%)
  matrix products  64.4 us (7%)
  local copies, waits for them, and re-layouts  18.5 us (2%)
  other arithmetic  13.4 us (1%)
  between operations  13.3 us (1%)
    all_gather x1, waiting for transfers between devices, body(): lax.all_gather(up_weight, 'sp', axis=0, tiled=True)  364 us
    all_gather x1, waiting for transfers between devices, body(): lax.all_gather(down_weight, 'sp', axis=1, tiled=True)  338 us
    reduce_scatter x1, waiting for transfers between devices, body(): lax.psum_scatter(partial_value.astype(jnp.bfloat16), 'tp', scatter_dimens...  58.3 us
    reduce_scatter x1, waiting for transfers between devices, body(): lax.psum_scatter(rounded(terms).astype(jnp.bfloat16), 'tp', scatter_dimen...  58 us
    all_gather x1, waiting for transfers between devices, body(): normed_whole = lax.all_gather(normed, 'tp', axis=1, tiled=True)  45.6 us
    dot_general x1, matrix products, body(): jnp.dot(activated, lax.all_gather(down_weight, 'sp', axis=1, tiled=True),...  25.8 us
    dot_general x1, matrix products, body(): jnp.dot(normed_whole, lax.all_gather(up_weight, 'sp', axis=0, tiled=True)...  25.8 us
  transfers between devices with their start and end apart: 6, of which 5 were waited for; matrix products, arithmetic and copies ran while one was open for 4% of the time, Pallas kernels for 0%

commit v1 on v0

--- a/solution.py
+++ b/solution.py
@@ -2,6 +2,7 @@
 import jax.numpy as jnp
 from jax import lax
 from jax.sharding import PartitionSpec as P
+from jax.lax import all_to_all, psum
 
 D = 3072
 HEAD_SIZE = 64
@@ -95,10 +96,11 @@
         preferred_element_type=jnp.float32,
     )
     activated = jnp.square(jax.nn.relu(hidden_pre)).astype(jnp.bfloat16)
+    fill_roots_in = lambda my_data, mesh_ax: jnp.concatenate(
+        all_to_all(jnp.stack([my_data] * psum(1, mesh_ax)), mesh_ax, 0, 0), axis=1
+    )
     terms = jnp.dot(
-        activated,
-        lax.all_gather(down_weight, "sp", axis=1, tiled=True),
-        preferred_element_type=jnp.float32,
+        activated, fill_roots_in(down_weight, mesh_ax="sp"), preferred_element_type=jnp.float32
     )
     branch_sum = lax.psum_scatter(
         rounded(terms).astype(jnp.bfloat16), "tp", scatter_dimension=1, tiled=True

time: 986 us -> 877 us (0.89)
  waiting for transfers between devices: 865 us -> 748 us
    all_gather x1 -> x0, waiting for transfers between devices: 338 us -> none  [body(): lax.all_gather(down_weight, 'sp', axis=1, tiled=True)]
    all_gather x1, waiting for transfers between devices: 364 us -> 590 us  [body(): lax.all_gather(up_weight, 'sp', axis=0, tiled=True)]
    all_gather x1, waiting for transfers between devices: 45.6 us -> 26.9 us  [body(): normed_whole = lax.all_gather(normed, 'tp', axis=1, tiled=True)]
    reduce_scatter x1, waiting for transfers between devices: 58 us -> 71.6 us  [body(): lax.psum_scatter(rounded(terms).astype(jnp.bfloat16), 'tp', scatter_dimen...]
  transfers between devices with their start and end apart: 6 -> 6, of which waited for: 5 -> 4; matrix products, arithmetic and copies ran while one was open for 4% -> 5% of each run, Pallas kernels for 0% -> 0%
where the time goes in v1:
time: 877 us
  waiting for transfers between devices  748 us (85%)
  matrix products  61.6 us (7%)
  local copies, waits for them, and re-layouts  24.9 us (3%)
  between operations  13.3 us (2%)
  other arithmetic  11.9 us (1%)
  starting transfers between devices  11.1 us (1%)
    all_gather x1, waiting for transfers between devices, body(): lax.all_gather(up_weight, 'sp', axis=0, tiled=True)  590 us
    reduce_scatter x1, waiting for transfers between devices, body(): lax.psum_scatter(rounded(terms).astype(jnp.bfloat16), 'tp', scatter_dimen...  71.6 us
    reduce_scatter x1, waiting for transfers between devices, body(): lax.psum_scatter(partial_value.astype(jnp.bfloat16), 'tp', scatter_dimens...  58.3 us
    all_gather x1, waiting for transfers between devices, body(): normed_whole = lax.all_gather(normed, 'tp', axis=1, tiled=True)  26.9 us
    dot_general x1, matrix products, body(): jnp.dot(activated, fill_roots_in(down_weight, mesh_ax='sp'), preferred_el...  25.9 us
    dot_general x1, matrix products, body(): jnp.dot(normed_whole, lax.all_gather(up_weight, 'sp', axis=0, tiled=True)...  25.7 us
  transfers between devices with their start and end apart: 6, of which 4 were waited for; matrix products, arithmetic and copies ran while one was open for 5% of the time, Pallas kernels for 0%

profile of v1, /device:TPU:0, one launch (start us, length us, event | category | flops | bytes accessed | tf_op | source)
XLA Modules:
  0.0 876.6 jit_solution(13488720457461711960)
XLA Ops:
  6.5 0.9 slice.32
  7.5 0.8 slice.33
  8.2 4.9 collective-permute-start
  13.1 0.1 add_compare_fusion
  13.3 1.0 broadcast_and_fusion
  14.3 1.2 reshape.101
  15.5 1.2 reshape.99
  16.7 0.7 max.26
  17.4 1.0 copy.19
  18.4 1.0 copy.15
  19.4 1.4 copy.20
  20.8 1.1 copy.36
  21.8 0.0 collective-permute-done
  21.9 1.1 pad_maximum_fusion
  23.0 0.2 reshape.100
  23.2 1.0 copy.18
  24.2 0.2 reshape.98
  24.4 0.4 copy.14
  24.8 2.5 fusion
  27.3 0.1 broadcast_maximum_fusion
  27.4 1.8 fusion.1
  29.2 0.1 exponential_add_fusion
  29.3 2.2 fusion.8
  31.5 0.5 copy.23
  32.0 0.0 copy-start.5
  32.1 5.4 convolution_convert_fusion.1
  37.4 0.0 reduce-scatter.3.cloned.1.call-update
  37.5 0.0 all-gather.3.cloned.1.call-start
  37.5 58.3 %reduce-scatter.3.cloned.1.call-done = bf16[1024,768]{1,0:T(8,128)(2,1)} async-done(((bf16[1024,3072]{1,0:T(8,128)(2,1)}), bf16[1024,768]{1,0:T(8,128)(2,1)}) %reduce-scatter.3.cloned.1.call-update) | async-done | bytes 1572880 | tf_op jit(solution)/shard_map/reduce_scatter | solution.py:84
  95.8 2.3 add_convert_fusion
  98.1 0.0 copy-start.2
  98.1 0.4 fusion.2
  98.5 5.8 psum.7
  104.3 1.6 fusion.4
  105.9 0.0 all-gather.3.cloned.1.call-update
  105.9 0.0 all-gather.5.cloned.1.call-start
  105.9 0.7 all-gather.5.cloned.1.call-update
  106.6 4.3 copy.24
  110.9 9.1 %stack.2 = bf16[8,3072,384]{1,2,0:T(8,128)(2,1)} broadcast(bf16[3072,384]{0,1:T(8,128)(2,1)} %copy.24), dimensions={1,2} | broadcast | bytes 21233664 | tf_op jit(solution)/shard_map/stack | solution.py:100
  120.0 5.9 all-to-all-start
  125.9 0.2 reduce-scatter.5.cloned.1.call-start
  126.1 26.9 %all-gather.3.cloned.1.call-done = bf16[1024,3072]{1,0:T(8,128)(2,1)} async-done(((bf16[1024,768]{1,0:T(8,128)(2,1)}), bf16[1024,3072]{1,0:T(8,128)(2,1)}) %all-gather.3.cloned.1.call-update) | async-done | bytes 6291472 | tf_op jit(solution)/shard_map/all_gather | solution.py:92
  153.0 590.5 %all-gather.5.cloned.1.call-done = bf16[3072,3072]{1,0:T(8,128)(2,1)} async-done(((bf16[384,3072]{1,0:T(8,128)(2,1)}), bf16[3072,3072]{1,0:T(8,128)(2,1)}) %all-gather.5.cloned.1.call-update) | async-done | bytes 18874384 | tf_op jit(solution)/shard_map/all_gather | solution.py:95
  743.5 25.7 %multiply_convert_fusion.clone.4 = bf16[1024,3072]{1,0:T(8,128)(2,1)} fusion(bf16[1024,3072]{1,0:T(8,128)(2,1)} %all-gather.3.cloned.1.call-done, bf16[3072,3072]{1,0:T(8,128)(2,1)} %all-gather.5.cloned.1.call-done), kind=kOutput, calls=%fused_computation.clone.clone.clone.1 | convolution fusion | flops 19336790016 | bytes 31457280 | tf_op jit(solution)/shard_map/dot_general | solution.py:93
  769.2 25.9 %convolution_convert_fusion = bf16[1024,3072]{1,0:T(8,128)(2,1)} fusion(bf16[3072,3072]{0,1:T(8,128)(2,1)} %bitcast.9, bf16[1024,3072]{1,0:T(8,128)(2,1)} %multiply_convert_fusion.clone.4), kind=kOutput, calls=%fused_computation.4 | convolution fusion | flops 19330498560 | bytes 31457280 | tf_op jit(solution)/shard_map/dot_general | solution.py:102
  795.0 0.0 reduce-scatter.5.cloned.1.call-update
  795.1 71.6 %reduce-scatter.5.cloned.1.call-done = bf16[1024,768]{1,0:T(8,128)(2,1)} async-done(((bf16[1024,3072]{1,0:T(8,128)(2,1)}), bf16[1024,768]{1,0:T(8,128)(2,1)}) %reduce-scatter.5.cloned.1.call-update) | async-done | bytes 1572880 | tf_op jit(solution)/shard_map/reduce_scatter | solution.py:105
  866.7 3.4 fusion.5
  (19 shorter events, 0.1 us)
Async XLA Ops:
  6.5 25.5 %copy-start = (bf16[384,3072]{1,0:T(8,128)(2,1)S(1)}, bf16[384,3072]{1,0:T(8,128)(2,1)}, u32[]{:S(2)}) copy-start(bf16[384,3072]{1,0:T(8,128)(2,1)} %param.13) | copy-start | bytes 7077892
  6.5 89.3 %reduce-scatter.3.cloned.1.call-start = ((), (), s32[]{:S(2)}) async-start(), calls=%async_computation.3 | async-start | bytes 7864320 | tf_op jit(solution)/shard_map/reduce_scatter | solution.py:84
  8.2 13.6 %collective-permute-start = (bf16[128,256]{1,0:T(8,128)(2,1)S(1)}, bf16[128,256]{1,0:T(8,128)(2,1)S(1)}, u32[]{:S(2)}, u32[]{:S(2)}) collective-permute-start(bf16[128,256]{1,0:T(8,128)(2,1)S(1)} %pad_maximum_fusion.2), channel_id=1, source_target_pairs={{0,4},{4,8},{8,12},{12,16},{16,20},{20,24},{24,28},{1,5},{5,9},{9,... | collective-permute-start | bytes 196616 | tf_op jit(solution)/shard_map/ppermute | solution.py:16
  23.2 4.2 copy-start.3
  24.8 4.5 copy-start.4
  32.0 5.5 copy-start.5
  37.5 115.6 %all-gather.3.cloned.1.call-start = ((), (), s32[]{:S(2)}) async-start(), calls=%async_computation.4 | async-start | bytes 7864320 | tf_op jit(solution)/shard_map/all_gather | solution.py:92
  98.1 12.8 %copy-start.2 = (bf16[1024,768]{1,0:T(8,128)(2,1)}, bf16[1024,768]{1,0:T(8,128)(2,1)S(1)}, u32[]{:S(2)}) copy-start(bf16[1024,768]{1,0:T(8,128)(2,1)S(1)} %add_convert_fusion) | copy-start | bytes 4718596
  105.9 637.6 %all-gather.5.cloned.1.call-start = ((), (), s32[]{:S(2)}) async-start(), calls=%async_computation.5 | async-start | bytes 21233664 | tf_op jit(solution)/shard_map/all_gather | solution.py:95
  120.0 649.2 %all-to-all-start = ((bf16[8,3072,384]{1,2,0:T(8,128)(2,1)}), bf16[8,3072,384]{1,2,0:T(8,128)(2,1)}, u32[]{:S(2)}, u32[]{:S(2)}) async-start(bf16[8,3072,384]{1,2,0:T(8,128)(2,1)} %stack.2), calls=%async_computation.1 | async-start | bytes 37748736 | tf_op jit(solution)/shard_map/all_to_all | solution.py:100
  125.9 740.8 %reduce-scatter.5.cloned.1.call-start = ((), (), s32[]{:S(2)}) async-start(), calls=%async_computation.6 | async-start | bytes 7864320 | tf_op jit(solution)/shard_map/reduce_scatter | solution.py:105
  769.2 100.9 %copy-start.1 = (bf16[384,3072]{1,0:T(8,128)(2,1)S(1)}, bf16[384,3072]{1,0:T(8,128)(2,1)}, u32[]{:S(2)}) copy-start(bf16[384,3072]{1,0:T(8,128)(2,1)} %param.13) | copy-start | bytes 7077892
Sparse Core Ops, SparseCore 0:
  37.6 58.1 reduce-scatter.2
  106.0 46.9 all-gather.2
  154.6 588.8 all-gather.4
  795.2 71.4 reduce-scatter.4
